TPU v7x, 32 devices: a whole 2x2x4 slice. The times are simulated.
32 devices in a mesh: dp: 4 (over y, x), kv: 4 (over z), tp: 2 (over core).
Axes of the slice: x: 2, y: 2, z: 4, core: 2. Of those that a mesh axis runs over, the one named last changes fastest.
Arguments:
- tokens: bfloat16 [4, 1024, 1024], P('dp', 'kv', 'tp'), may hold values from -6 to 6
- norm_gain: float32 [1024], replicated, may hold values from 0.1 to 1.9
- w_query: bfloat16 [1024, 1024], P(None, 'tp'), may hold values from -0.1875 to 0.1875
- w_key: bfloat16 [1024, 256], P(None, 'tp'), may hold values from -0.1875 to 0.1875
- w_value: bfloat16 [1024, 256], P(None, 'tp'), may hold values from -0.1875 to 0.1875
- q_gain: float32 [64], replicated, may hold values from 0.1 to 1.9
- k_gain: float32 [64], replicated, may hold values from 0.1 to 1.9
- w_out: bfloat16 [1024, 1024], P('tp'), may hold values from -4 to 4
- chosen: int32 [4, 32, 16], P('dp', 'kv'), may hold values from -1 to 31, as said below
Outputs:
- mixed: bfloat16 [4, 1024, 1024], P('dp', 'kv', 'tp')
- log_total: float32 [4, 16, 1024], P('dp', 'tp', 'kv')
Inputs may be any that keep to these rules, and one draw needn't show every extreme that they name: Each row of chosen (one query block b) holds distinct key block numbers, all at most b, and -1 for empty entries; b itself is always present; a row is full (16 blocks) whenever at least 16 blocks may be chosen by it. Over the 8 rows of one index of kv, the chosen blocks that lie on any one other index of kv are at most 4 distinct ones, and exactly 4 of those on the index just before, for every index but the first. Some blocks are chosen far more often than others.
All inputs are finite; a program needn't handle non-finite values.
Results may differ from a plain program's by a relative error of at most 0.015.
Values may be sent and summed in bfloat16 or wider, within the bound.
A program may use at most 64 MiB of HBM per device.

v0:
```python
import math
import jax
import jax.numpy as jnp
from jax import lax
from jax.sharding import PartitionSpec as P

H = 16
HD = 64
BLK = 32
epsilon = 1e-06
alibi_reach = 4.0
masked = -1e30


def rms_norm(values, gain):
    return (
        values
        * lax.rsqrt(jnp.mean(values * values, axis=-1, keepdims=True) + epsilon)
        * gain.astype(jnp.float32)
    )


def shards(tokens, norm_gain, w_query, w_key, w_value, q_gain, k_gain, w_out, chosen):
    gathered = lax.all_gather(tokens, "tp", axis=2, tiled=True)
    seq_dev, tok_dev, model_width = gathered.shape
    n_kv = lax.axis_size("kv")
    n_tp = lax.axis_size("tp")
    kv_index = lax.axis_index("kv")
    tp_index = lax.axis_index("tp")
    heads_here = w_query.shape[1] // HD
    kv_here = w_key.shape[1] // HD
    group_size = heads_here // kv_here
    blocks_here = tok_dev // BLK
    seq_len = tok_dev * n_kv
    hidden = (
        rms_norm(gathered.astype(jnp.float32), norm_gain)
        .astype(jnp.bfloat16)
        .reshape(seq_dev * tok_dev, model_width)
    )
    queries = rms_norm(
        jnp.dot(hidden, w_query, preferred_element_type=jnp.float32).reshape(
            seq_dev, tok_dev, heads_here, HD
        ),
        q_gain,
    ).astype(jnp.bfloat16)
    key_rows = rms_norm(
        jnp.dot(hidden, w_key, preferred_element_type=jnp.float32).reshape(
            seq_dev, tok_dev, kv_here, HD
        ),
        k_gain,
    ).astype(jnp.bfloat16)
    value_rows = (
        jnp.dot(hidden, w_value, preferred_element_type=jnp.float32)
        .astype(jnp.bfloat16)
        .reshape(seq_dev, tok_dev, kv_here, HD)
    )
    queries = queries.reshape(seq_dev, blocks_here, BLK, kv_here, group_size, HD)
    head_ids = tp_index * heads_here + jnp.arange(heads_here, dtype=jnp.int32)
    slopes = jnp.exp2(-8.0 * (head_ids + 1).astype(jnp.float32) / H).reshape(kv_here, group_size)
    query_pos = (kv_index * tok_dev + jnp.arange(tok_dev, dtype=jnp.int32)).reshape(
        blocks_here, BLK
    )
    score_scale = HD ** (-0.5)

    def absorb(state_now, span_keys, span_values, key_pos, usable):
        row_max, row_sum, weighted = state_now
        key_block = key_pos // BLK
        member = jnp.any(chosen[:, :, :, None] == key_block[:, None, None, :], axis=2)
        offset = query_pos[None, :, :, None] - key_pos[:, None, None, :]
        allowed = member[:, :, None, :] & usable[:, None, None, :] & (offset >= 0)
        scores = (
            jnp.einsum(
                "sbqkgd,snkd->skgbqn", queries, span_keys, preferred_element_type=jnp.float32
            )
            * score_scale
        )
        penalty = (
            slopes[None, :, :, None, None, None]
            * offset.astype(jnp.float32)[:, None, None]
            * alibi_reach
            / seq_len
        )
        scores = jnp.where(allowed[:, None, None], scores - penalty, masked)
        new_max = jnp.maximum(row_max, jnp.max(scores, axis=-1))
        weights = jnp.where(allowed[:, None, None], jnp.exp(scores - new_max[..., None]), 0.0)
        shrink = jnp.exp(row_max - new_max)
        row_sum = row_sum * shrink + jnp.sum(weights, axis=-1)
        weighted = weighted * shrink[..., None] + jnp.einsum(
            "skgbqn,snkd->skgbqd",
            weights.astype(jnp.bfloat16),
            span_values,
            preferred_element_type=jnp.float32,
        )
        return (new_max, row_sum, weighted)

    stat_shape = (seq_dev, kv_here, group_size, blocks_here, BLK)
    initial = (
        jnp.full(stat_shape, masked, jnp.float32),
        jnp.zeros(stat_shape, jnp.float32),
        jnp.zeros(stat_shape + (HD,), jnp.float32),
    )

    def fold_piece(state_now, shard_piece, first_row):
        piece_keys, piece_values = shard_piece
        row_count = piece_keys.shape[1]
        span_len = math.gcd(row_count, tok_dev)

        def one_span(step_index, running):
            first_key = step_index * span_len
            span_keys = lax.dynamic_slice_in_dim(piece_keys, first_key, span_len, 1)
            span_values = lax.dynamic_slice_in_dim(piece_values, first_key, span_len, 1)
            key_pos = jnp.broadcast_to(
                first_row.astype(jnp.int32) + first_key + jnp.arange(span_len, dtype=jnp.int32),
                (seq_dev, span_len),
            )
            return absorb(
                running, span_keys, span_values, key_pos, jnp.ones((seq_dev, span_len), bool)
            )

        return lax.fori_loop(0, row_count // span_len, one_span, state_now)

    row_max, row_sum, weighted = fold_piece(
        initial,
        (
            lax.all_gather(key_rows, "kv", axis=1, tiled=True),
            lax.all_gather(value_rows, "kv", axis=1, tiled=True),
        ),
        jnp.int32(0),
    )
    attended = (weighted / row_sum[..., None]).transpose(0, 3, 4, 1, 2, 5)
    attended = attended.reshape(seq_dev * tok_dev, heads_here * HD).astype(jnp.bfloat16)
    log_total = (row_max + jnp.log(row_sum)).reshape(seq_dev, heads_here, tok_dev)
    own_rows = model_width // n_tp

    def project():
        out_cols = lax.slice_in_dim(w_out, 0, own_rows * lax.axis_size("tp"), axis=1)
        return jnp.dot(attended, out_cols, preferred_element_type=jnp.float32).T

    scattered = lax.psum_scatter(
        project().astype(jnp.bfloat16), "tp", scatter_dimension=0, tiled=True
    ).astype(jnp.float32)
    mixed = scattered.T.reshape(seq_dev, tok_dev, own_rows).astype(jnp.bfloat16)
    return (mixed, log_total)


def solution(mesh):
    in_specs = (
        P("dp", "kv", "tp"),
        P(),
        P(None, "tp"),
        P(None, "tp"),
        P(None, "tp"),
        P(),
        P(),
        P("tp", None),
        P("dp", "kv", None),
    )
    out_specs = (P("dp", "kv", "tp"), P("dp", "tp", "kv"))
    return jax.shard_map(shards, mesh=mesh, in_specs=in_specs, out_specs=out_specs, check_vma=False)
```

profile of v0, /device:TPU:0, one launch (start us, length us, event | category | flops | bytes accessed | tf_op | source)
XLA Modules:
  0.0 81.3 jit_solution(10249953948225324526)
XLA Ops:
  7.3 2.6 %all_gather.9 = bf16[1,256,1024]{2,1,0:T(8,128)(2,1)S(1)} all-gather(bf16[1,256,512]{2,1,0:T(8,128)(2,1)} %param.11), channel_id=1, replica_groups=mesh['dp'=4,'kv'=4,'tp'=2] {'tp'}, dimensions={2}, use_global_device_ids=true | all-gather | bytes 786432 | tf_op jit(solution)/shard_map/all_gather | solution.py:24
  9.9 0.2 fusion.20
  10.1 1.4 %convolution_convert_fusion.1 = bf16[256,128]{0,1:T(8,128)(2,1)S(1)} fusion(bf16[1024,128]{1,0:T(8,128)(2,1)} %param.15, bf16[1,256,1024]{2,1,0:T(8,128)(2,1)S(1)} %all_gather.9, f32[1024]{0:T(1024)} %param.12, f32[256]{0:T(256)S(1)} %add_rsqrt_fusion.2), kind=kOutput, calls=%fused_computation.39 | convolution fusion | flops 68190208 | bytes 857088 | tf_op jit(solution)/shard_map/dot_general | solution.py:53
  11.5 0.4 fusion.30
  12.0 16.2 %all_gather.10 = bf16[1,1024,2,64]{1,3,2,0:T(8,128)(2,1)} all-gather(bf16[1,256,2,64]{1,3,2,0:T(8,128)(2,1)S(1)} %multiply_convert_fusion), channel_id=1, replica_groups=mesh['dp'=4,'kv'=4,'tp'=2] {'kv'}, dimensions={1}, use_global_device_ids=true | all-gather | bytes 327680 | tf_op jit(solution)/shard_map/all_gather | solution.py:125
  28.2 14.6 %all_gather.11 = bf16[1,1024,2,64]{1,3,2,0:T(8,128)(2,1)S(1)} all-gather(bf16[1,256,2,64]{1,3,2,0:T(8,128)(2,1)S(1)} %bitcast.99), channel_id=1, replica_groups=mesh['dp'=4,'kv'=4,'tp'=2] {'kv'}, dimensions={1}, use_global_device_ids=true | all-gather | bytes 327680 | tf_op jit(solution)/shard_map/all_gather | solution.py:126
  42.8 1.3 %fusion.33 = (f32[256,512]{1,0:T(8,128)S(1)}, f32[256,512]{1,0:T(8,128)}) fusion(bf16[1024,512]{1,0:T(8,128)(2,1)S(1)} %copy-done, bf16[1,256,1024]{2,1,0:T(8,128)(2,1)S(1)} %all_gather.9, f32[1024]{0:T(1024)S(1)} %copy-done.3, f32[256]{0:T(256)S(1)} %add_rsqrt_fusion.2), kind=kOutput, calls=%fused_computation.59 | convolution fusion | flops 269615104 | bytes 2626560 | tf_op jit(solution)/shard_map/dot_general | solution.py:41
  44.1 0.2 copy.26
  44.5 1.6 %reshape.336 = f32[1,8,32,2,4,64]{5,4,3,2,1,0:T(4,128)S(1)} reshape(f32[256,512]{1,0:T(8,128)} %get-tuple-element.319) | data formatting | bytes 1048576 | tf_op jit(solution)/shard_map/reshape | solution.py:41
  46.1 1.1 %fusion.24 = bf16[1,8,32,2,4,64]{5,2,4,1,3,0:T(8,128)(2,1)} fusion(f32[1,8,32,2,4,64]{5,4,3,2,1,0:T(4,128)S(1)} %reshape.336, f32[64]{0:T(128)S(1)} %copy-done.5, f32[8,32,2,4]{1,3,0,2:T(4,128)S(1)} %copy.27), kind=kLoop, calls=%fused_computation.45 | loop fusion | flops 393216 | bytes 794880 | tf_op jit(solution)/shard_map/convert_element_type | solution.py:45
  47.2 15.7 %while.20 = (s32[]{:T(128)}, f32[1,2,4,8,32]{4,2,3,1,0:T(4,128)S(1)}, f32[1,2,4,8,32]{4,2,3,1,0:T(4,128)S(1)}, f32[1,2,4,8,32,64]{5,4,3,2,1,0:T(8,128)S(1)}, s32...) while((s32[]{:T(128)}, ...), condition=%wide.region_7.8_spmd.clone, body=%wide.region_3.7_spmd.clone.sunk | while | flops 140261664 | bytes 9419611 | solution.py:120
  47.5 0.1 fusion.48
  47.8 1.7 %fusion.49 = (f32[2,4,8,32]{3,1,2,0:T(4,128)S(1)}, f32[1,2,4,8,32,256]{5,4,2,3,1,0:T(8,128)S(1)}) fusion(f32[8,32,256]{2,1,0:T(8,128)S(1)} %subtract_convert_fusion.2, f32[2,4]{1,0:T(2,128)S(1)} %mul.331, bf16[1,8,32,2,4,64]{5,2,4,1,3,0:T(8,128)(2,1)} %get-tuple-element.431, bf16[1,1024,2,64]{1,3,2,0:T(8,128)(2,1)} %get-tuple-element.430, ...), kind=kOutput, calls=%fused_computation.58.clone.1 | convolution fusion | flops 70252544 | bytes 3022884 | tf_op jit(solution)/shard_map/while/body/eval_jaxpr/sbqkgd,snkd->skgbqn/dot_general | solution.py:72
  49.6 0.8 %fusion.51 = (bf16[2,4,8,32,256]{4,3,1,2,0:T(8,128)(2,1)S(1)}, f32[2,4,8,32]{3,1,2,0:T(4,128)S(1)}) fusion(f32[1,2,4,8,32,256]{5,4,2,3,1,0:T(8,128)S(1)} %get-tuple-element.393, f32[2,4,8,32]{3,1,2,0:T(4,128)S(1)} %bitcast.92, pred[8,32,256]{2,1,0:T(8,128)(4,1)S(1)} %fusion.48), kind=kLoop, calls=%fused_computation.9.clone.1 | loop fusion | flops 2095104 | bytes 3227648 | tf_op jit(solution)/shard_map/reshape.263
  50.4 0.7 fusion.52
  51.5 0.1 fusion.48
  51.7 1.7 %fusion.49 = (f32[2,4,8,32]{3,1,2,0:T(4,128)S(1)}, f32[1,2,4,8,32,256]{5,4,2,3,1,0:T(8,128)S(1)}) fusion(f32[8,32,256]{2,1,0:T(8,128)S(1)} %subtract_convert_fusion.2, f32[2,4]{1,0:T(2,128)S(1)} %mul.331, bf16[1,8,32,2,4,64]{5,2,4,1,3,0:T(8,128)(2,1)} %get-tuple-element.431, bf16[1,1024,2,64]{1,3,2,0:T(8,128)(2,1)} %get-tuple-element.430, ...), kind=kOutput, calls=%fused_computation.58.clone.1 | convolution fusion | flops 70252544 | bytes 3022884 | tf_op jit(solution)/shard_map/while/body/eval_jaxpr/sbqkgd,snkd->skgbqn/dot_general | solution.py:72
  53.5 0.8 %fusion.51 = (bf16[2,4,8,32,256]{4,3,1,2,0:T(8,128)(2,1)S(1)}, f32[2,4,8,32]{3,1,2,0:T(4,128)S(1)}) fusion(f32[1,2,4,8,32,256]{5,4,2,3,1,0:T(8,128)S(1)} %get-tuple-element.393, f32[2,4,8,32]{3,1,2,0:T(4,128)S(1)} %bitcast.92, pred[8,32,256]{2,1,0:T(8,128)(4,1)S(1)} %fusion.48), kind=kLoop, calls=%fused_computation.9.clone.1 | loop fusion | flops 2095104 | bytes 3227648 | tf_op jit(solution)/shard_map/reshape.263
  54.4 0.6 fusion.52
  55.6 1.7 %fusion.49 = (f32[2,4,8,32]{3,1,2,0:T(4,128)S(1)}, f32[1,2,4,8,32,256]{5,4,2,3,1,0:T(8,128)S(1)}) fusion(f32[8,32,256]{2,1,0:T(8,128)S(1)} %subtract_convert_fusion.2, f32[2,4]{1,0:T(2,128)S(1)} %mul.331, bf16[1,8,32,2,4,64]{5,2,4,1,3,0:T(8,128)(2,1)} %get-tuple-element.431, bf16[1,1024,2,64]{1,3,2,0:T(8,128)(2,1)} %get-tuple-element.430, ...), kind=kOutput, calls=%fused_computation.58.clone.1 | convolution fusion | flops 70252544 | bytes 3022884 | tf_op jit(solution)/shard_map/while/body/eval_jaxpr/sbqkgd,snkd->skgbqn/dot_general | solution.py:72
  57.4 0.8 %fusion.51 = (bf16[2,4,8,32,256]{4,3,1,2,0:T(8,128)(2,1)S(1)}, f32[2,4,8,32]{3,1,2,0:T(4,128)S(1)}) fusion(f32[1,2,4,8,32,256]{5,4,2,3,1,0:T(8,128)S(1)} %get-tuple-element.393, f32[2,4,8,32]{3,1,2,0:T(4,128)S(1)} %bitcast.92, pred[8,32,256]{2,1,0:T(8,128)(4,1)S(1)} %fusion.48), kind=kLoop, calls=%fused_computation.9.clone.1 | loop fusion | flops 2095104 | bytes 3227648 | tf_op jit(solution)/shard_map/reshape.263
  58.3 0.6 fusion.52
  59.3 0.1 fusion.48
  59.5 1.7 %fusion.49 = (f32[2,4,8,32]{3,1,2,0:T(4,128)S(1)}, f32[1,2,4,8,32,256]{5,4,2,3,1,0:T(8,128)S(1)}) fusion(f32[8,32,256]{2,1,0:T(8,128)S(1)} %subtract_convert_fusion.2, f32[2,4]{1,0:T(2,128)S(1)} %mul.331, bf16[1,8,32,2,4,64]{5,2,4,1,3,0:T(8,128)(2,1)} %get-tuple-element.431, bf16[1,1024,2,64]{1,3,2,0:T(8,128)(2,1)} %get-tuple-element.430, ...), kind=kOutput, calls=%fused_computation.58.clone.1 | convolution fusion | flops 70252544 | bytes 3022884 | tf_op jit(solution)/shard_map/while/body/eval_jaxpr/sbqkgd,snkd->skgbqn/dot_general | solution.py:72
  61.3 0.8 %fusion.51 = (bf16[2,4,8,32,256]{4,3,1,2,0:T(8,128)(2,1)S(1)}, f32[2,4,8,32]{3,1,2,0:T(4,128)S(1)}) fusion(f32[1,2,4,8,32,256]{5,4,2,3,1,0:T(8,128)S(1)} %get-tuple-element.393, f32[2,4,8,32]{3,1,2,0:T(4,128)S(1)} %bitcast.92, pred[8,32,256]{2,1,0:T(8,128)(4,1)S(1)} %fusion.48), kind=kLoop, calls=%fused_computation.9.clone.1 | loop fusion | flops 2095104 | bytes 3227648 | tf_op jit(solution)/shard_map/reshape.263
  62.2 0.7 fusion.52
  62.9 0.3 fusion.26
  63.3 0.4 copy.30
  63.7 0.3 convert_element_type.92
  64.1 1.2 %fusion.19 = bf16[1024,256]{0,1:T(8,128)(2,1)} fusion(bf16[256,512]{1,0:T(8,128)(2,1)S(1)} %convert_element_type.92, bf16[512,1024]{1,0:T(8,128)(2,1)S(1)} %copy-done.1), kind=kOutput, calls=%fused_computation.38 | convolution fusion | flops 268697600 | bytes 1835008 | tf_op jit(solution)/shard_map/dot_general | solution.py:137
  65.4 0.7 reshape.338
  66.1 8.4 %reduce-scatter.2.cloned.1.call-done = bf16[512,256]{0,1:T(8,128)(2,1)} async-done(((bf16[1024,256]{0,1:T(8,128)(2,1)}), bf16[512,256]{0,1:T(8,128)(2,1)}) %reduce-scatter.2.cloned.1.call-update) | async-done | bytes 262160 | tf_op jit(solution)/shard_map/reduce_scatter | solution.py:139
  (75 shorter events, 2.5 us)
Async XLA Ops:
  7.2 35.7 %copy-start = (bf16[1024,512]{1,0:T(8,128)(2,1)S(1)}, bf16[1024,512]{1,0:T(8,128)(2,1)}, u32[]{:S(2)}) copy-start(bf16[1024,512]{1,0:T(8,128)(2,1)} %param.13) | copy-start | bytes 3145732
  7.2 4.3 %copy-start.3 = (f32[1024]{0:T(1024)S(1)}, f32[1024]{0:T(1024)}, u32[]{:S(2)}) copy-start(f32[1024]{0:T(1024)} %param.12) | copy-start | bytes 12292
  7.2 4.3 %copy-start.6 = (bf16[1024,128]{1,0:T(8,128)(2,1)S(1)}, bf16[1024,128]{1,0:T(8,128)(2,1)}, u32[]{:S(2)}) copy-start(bf16[1024,128]{1,0:T(8,128)(2,1)} %param.14) | copy-start | bytes 786436
  7.2 4.7 %copy-start.4 = (f32[64]{0:T(128)S(1)}, f32[64]{0:T(128)}, u32[]{:S(2)}) copy-start(f32[64]{0:T(128)} %param.17) | copy-start | bytes 772
  7.2 67.2 %reduce-scatter.2.cloned.1.call-start = ((), (), s32[]{:S(2)}) async-start(), calls=%async_computation.1 | async-start | bytes 786432 | tf_op jit(solution)/shard_map/reduce_scatter | solution.py:139
  44.1 2.0 %copy-start.5 = (f32[64]{0:T(128)S(1)}, f32[64]{0:T(128)}, u32[]{:S(2)}) copy-start(f32[64]{0:T(128)} %param.16) | copy-start | bytes 772
  44.3 2.9 %copy-start.2 = (s32[1,8,16]{2,1,0:T(8,128)S(1)}, s32[1,8,16]{2,1,0:T(8,128)}, u32[]{:S(2)}) copy-start(s32[1,8,16]{2,1,0:T(8,128)} %param.19) | copy-start | bytes 1540
  62.9 1.2 %copy-start.1 = (bf16[512,1024]{1,0:T(8,128)(2,1)S(1)}, bf16[512,1024]{1,0:T(8,128)(2,1)}, u32[]{:S(2)}) copy-start(bf16[512,1024]{1,0:T(8,128)(2,1)} %param.18) | copy-start | bytes 3145732
Sparse Core Ops, SparseCore 0:
  65.5 8.8 reduce-scatter.1
where the time goes:
time: 81.6 us; the launch traced here: 81.3 us
  blocking collectives  33.4 us (41%)
  between operations  14.3 us (18%)
  matrix products  13.8 us (17%)
  waiting for transfers between devices  8.37 us (10%)
  other arithmetic  6.92 us (8%)
  local copies, waits for them, and re-layouts  4.09 us (5%)
    all_gather x1, blocking collectives, shards(): lax.all_gather(key_rows, 'kv', axis=1, tiled=True)  16.2 us
    all_gather x1, blocking collectives, shards(): lax.all_gather(value_rows, 'kv', axis=1, tiled=True)  14.6 us
    reduce_scatter x1, waiting for transfers between devices, shards(): lax.psum_scatter(project().astype(jnp.bfloat16), 'tp', scatter_dimension=...  8.35 us
    dot_general x4, matrix products, absorb(): jnp.einsum('sbqkgd,snkd->skgbqn', queries, span_keys, preferred_element_t...  6.99 us
    another operation x4, other arithmetic  3.33 us
    all_gather x1, blocking collectives, shards(): gathered = lax.all_gather(tokens, 'tp', axis=2, tiled=True)  2.64 us
    dot_general x4, matrix products, absorb(): jnp.einsum('skgbqn,snkd->skgbqd', weights.astype(jnp.bfloat16), span_valu...  2.6 us
  transfers between devices with their start and end apart: 1, of which 1 were waited for; matrix products, arithmetic and copies ran while one was open for 1% of the time, Pallas kernels for 0%

commit v1 on v0

--- a/solution.py
+++ b/solution.py
@@ -10,6 +10,12 @@
 epsilon = 1e-06
 alibi_reach = 4.0
 masked = -1e30
+
+
+def enter_sides(z_in, out_dim):
+    right_arr = lax.all_gather(z_in, axis_name="kv")
+    seen_now = jnp.concatenate(right_arr, axis=out_dim)
+    return seen_now
 
 
 def rms_norm(values, gain):
@@ -121,10 +127,7 @@
 
     row_max, row_sum, weighted = fold_piece(
         initial,
-        (
-            lax.all_gather(key_rows, "kv", axis=1, tiled=True),
-            lax.all_gather(value_rows, "kv", axis=1, tiled=True),
-        ),
+        (lax.all_gather(key_rows, "kv", axis=1, tiled=True), enter_sides(value_rows, out_dim=1)),
         jnp.int32(0),
     )
     attended = (weighted / row_sum[..., None]).transpose(0, 3, 4, 1, 2, 5)

time: 81.6 us -> 81.7 us (level)
  no operation moved by 1% of the time
where the time goes in v1:
time: 81.7 us; the launch traced here: 81.4 us
  blocking collectives  33.4 us (41%)
  between operations  14.3 us (18%)
  matrix products  13.9 us (17%)
  waiting for transfers between devices  8.4 us (10%)
  other arithmetic  6.92 us (8%)
  local copies, waits for them, and re-layouts  4.12 us (5%)
    all_gather x1, blocking collectives, shards(): lax.all_gather(key_rows, 'kv', axis=1, tiled=True)  16.2 us
    all_gather x1, blocking collectives, enter_sides(): right_arr = lax.all_gather(z_in, axis_name='kv')  14.6 us
    reduce_scatter x1, waiting for transfers between devices, shards(): lax.psum_scatter(project().astype(jnp.bfloat16), 'tp', scatter_dimension=...  8.38 us
    dot_general x4, matrix products, absorb(): jnp.einsum('sbqkgd,snkd->skgbqn', queries, span_keys, preferred_element_t...  6.99 us
    another operation x4, other arithmetic  3.33 us
    all_gather x1, blocking collectives, shards(): gathered = lax.all_gather(tokens, 'tp', axis=2, tiled=True)  2.64 us
    dot_general x4, matrix products, absorb(): jnp.einsum('skgbqn,snkd->skgbqd', weights.astype(jnp.bfloat16), span_valu...  2.62 us
  transfers between devices with their start and end apart: 1, of which 1 were waited for; matrix products, arithmetic and copies ran while one was open for 1% of the time, Pallas kernels for 0%

profile of v1, /device:TPU:0, one launch (start us, length us, event | category | flops | bytes accessed | tf_op | source)
XLA Modules:
  0.0 81.4 jit_solution(15955463828684804810)
XLA Ops:
  7.3 2.6 %all_gather.9 = bf16[1,256,1024]{2,1,0:T(8,128)(2,1)S(1)} all-gather(bf16[1,256,512]{2,1,0:T(8,128)(2,1)} %param.11), channel_id=1, replica_groups=mesh['dp'=4,'kv'=4,'tp'=2] {'tp'}, dimensions={2}, use_global_device_ids=true | all-gather | bytes 786432 | tf_op jit(solution)/shard_map/all_gather | solution.py:30
  9.9 0.2 fusion.20
  10.1 1.4 %convolution_convert_fusion.1 = bf16[256,128]{0,1:T(8,128)(2,1)S(1)} fusion(bf16[1024,128]{1,0:T(8,128)(2,1)} %param.15, bf16[1,256,1024]{2,1,0:T(8,128)(2,1)S(1)} %all_gather.9, f32[1024]{0:T(1024)} %param.12, f32[256]{0:T(256)S(1)} %add_rsqrt_fusion.2), kind=kOutput, calls=%fused_computation.39 | convolution fusion | flops 68190208 | bytes 857088 | tf_op jit(solution)/shard_map/dot_general | solution.py:59
  11.5 0.4 fusion.30
  12.0 16.2 %all_gather.10 = bf16[1,1024,2,64]{1,3,2,0:T(8,128)(2,1)} all-gather(bf16[1,256,2,64]{1,3,2,0:T(8,128)(2,1)S(1)} %multiply_convert_fusion), channel_id=1, replica_groups=mesh['dp'=4,'kv'=4,'tp'=2] {'kv'}, dimensions={1}, use_global_device_ids=true | all-gather | bytes 327680 | tf_op jit(solution)/shard_map/all_gather | solution.py:130
  28.3 14.6 %all_gather.11 = bf16[4,1,256,2,64]{2,4,3,1,0:T(8,128)(2,1)S(1)} all-gather(bf16[1,1,256,2,64]{2,4,3,1,0:T(8,128)(2,1)S(1)} %bitcast.103), channel_id=1, replica_groups=mesh['dp'=4,'kv'=4,'tp'=2] {'kv'}, dimensions={0}, use_global_device_ids=true | all-gather | bytes 327680 | tf_op jit(solution)/shard_map/all_gather | solution.py:16
  42.9 1.3 %fusion.33 = (f32[256,512]{1,0:T(8,128)S(1)}, f32[256,512]{1,0:T(8,128)}) fusion(bf16[1024,512]{1,0:T(8,128)(2,1)S(1)} %copy-done, bf16[1,256,1024]{2,1,0:T(8,128)(2,1)S(1)} %all_gather.9, f32[1024]{0:T(1024)S(1)} %copy-done.3, f32[256]{0:T(256)S(1)} %add_rsqrt_fusion.2), kind=kOutput, calls=%fused_computation.59 | convolution fusion | flops 269615104 | bytes 2626560 | tf_op jit(solution)/shard_map/dot_general | solution.py:47
  44.2 0.2 copy.45
  44.5 1.6 %reshape.336 = f32[1,8,32,2,4,64]{5,4,3,2,1,0:T(4,128)S(1)} reshape(f32[256,512]{1,0:T(8,128)} %get-tuple-element.319) | data formatting | bytes 1048576 | tf_op jit(solution)/shard_map/reshape | solution.py:47
  46.1 1.1 %fusion.24 = bf16[1,8,32,2,4,64]{5,2,4,1,3,0:T(8,128)(2,1)} fusion(f32[1,8,32,2,4,64]{5,4,3,2,1,0:T(4,128)S(1)} %reshape.336, f32[64]{0:T(128)S(1)} %copy-done.5, f32[8,32,2,4]{1,3,0,2:T(4,128)S(1)} %copy.46), kind=kLoop, calls=%fused_computation.45 | loop fusion | flops 393216 | bytes 794880 | tf_op jit(solution)/shard_map/convert_element_type | solution.py:51
  47.3 15.7 %while.20 = (s32[]{:T(128)}, f32[1,2,4,8,32]{4,2,3,1,0:T(4,128)S(1)}, f32[1,2,4,8,32]{4,2,3,1,0:T(4,128)S(1)}, f32[1,2,4,8,32,64]{5,4,3,2,1,0:T(8,128)S(1)}, s32...) while((s32[]{:T(128)}, ...), condition=%wide.region_7.8_spmd.clone, body=%wide.region_3.7_spmd.clone.sunk | while | flops 140261664 | bytes 9419611 | solution.py:126
  47.6 0.1 fusion.48
  47.8 1.7 %fusion.49 = (f32[2,4,8,32]{3,1,2,0:T(4,128)S(1)}, f32[1,2,4,8,32,256]{5,4,2,3,1,0:T(8,128)S(1)}) fusion(f32[8,32,256]{2,1,0:T(8,128)S(1)} %subtract_convert_fusion.2, f32[2,4]{1,0:T(2,128)S(1)} %mul.331, bf16[1,8,32,2,4,64]{5,2,4,1,3,0:T(8,128)(2,1)} %get-tuple-element.431, bf16[1,1024,2,64]{1,3,2,0:T(8,128)(2,1)} %get-tuple-element.430, ...), kind=kOutput, calls=%fused_computation.58.clone.1 | convolution fusion | flops 70252544 | bytes 3022884 | tf_op jit(solution)/shard_map/while/body/eval_jaxpr/sbqkgd,snkd->skgbqn/dot_general | solution.py:78
  49.6 0.8 %fusion.51 = (bf16[2,4,8,32,256]{4,3,1,2,0:T(8,128)(2,1)S(1)}, f32[2,4,8,32]{3,1,2,0:T(4,128)S(1)}) fusion(f32[1,2,4,8,32,256]{5,4,2,3,1,0:T(8,128)S(1)} %get-tuple-element.393, f32[2,4,8,32]{3,1,2,0:T(4,128)S(1)} %bitcast.94, pred[8,32,256]{2,1,0:T(8,128)(4,1)S(1)} %fusion.48), kind=kLoop, calls=%fused_computation.9.clone.1 | loop fusion | flops 2095104 | bytes 3227648 | tf_op jit(solution)/shard_map/reshape.263
  50.5 0.6 fusion.52
  51.5 0.1 fusion.48
  51.7 1.7 %fusion.49 = (f32[2,4,8,32]{3,1,2,0:T(4,128)S(1)}, f32[1,2,4,8,32,256]{5,4,2,3,1,0:T(8,128)S(1)}) fusion(f32[8,32,256]{2,1,0:T(8,128)S(1)} %subtract_convert_fusion.2, f32[2,4]{1,0:T(2,128)S(1)} %mul.331, bf16[1,8,32,2,4,64]{5,2,4,1,3,0:T(8,128)(2,1)} %get-tuple-element.431, bf16[1,1024,2,64]{1,3,2,0:T(8,128)(2,1)} %get-tuple-element.430, ...), kind=kOutput, calls=%fused_computation.58.clone.1 | convolution fusion | flops 70252544 | bytes 3022884 | tf_op jit(solution)/shard_map/while/body/eval_jaxpr/sbqkgd,snkd->skgbqn/dot_general | solution.py:78
  53.5 0.8 %fusion.51 = (bf16[2,4,8,32,256]{4,3,1,2,0:T(8,128)(2,1)S(1)}, f32[2,4,8,32]{3,1,2,0:T(4,128)S(1)}) fusion(f32[1,2,4,8,32,256]{5,4,2,3,1,0:T(8,128)S(1)} %get-tuple-element.393, f32[2,4,8,32]{3,1,2,0:T(4,128)S(1)} %bitcast.94, pred[8,32,256]{2,1,0:T(8,128)(4,1)S(1)} %fusion.48), kind=kLoop, calls=%fused_computation.9.clone.1 | loop fusion | flops 2095104 | bytes 3227648 | tf_op jit(solution)/shard_map/reshape.263
  54.4 0.7 fusion.52
  55.7 1.7 %fusion.49 = (f32[2,4,8,32]{3,1,2,0:T(4,128)S(1)}, f32[1,2,4,8,32,256]{5,4,2,3,1,0:T(8,128)S(1)}) fusion(f32[8,32,256]{2,1,0:T(8,128)S(1)} %subtract_convert_fusion.2, f32[2,4]{1,0:T(2,128)S(1)} %mul.331, bf16[1,8,32,2,4,64]{5,2,4,1,3,0:T(8,128)(2,1)} %get-tuple-element.431, bf16[1,1024,2,64]{1,3,2,0:T(8,128)(2,1)} %get-tuple-element.430, ...), kind=kOutput, calls=%fused_computation.58.clone.1 | convolution fusion | flops 70252544 | bytes 3022884 | tf_op jit(solution)/shard_map/while/body/eval_jaxpr/sbqkgd,snkd->skgbqn/dot_general | solution.py:78
  57.5 0.8 %fusion.51 = (bf16[2,4,8,32,256]{4,3,1,2,0:T(8,128)(2,1)S(1)}, f32[2,4,8,32]{3,1,2,0:T(4,128)S(1)}) fusion(f32[1,2,4,8,32,256]{5,4,2,3,1,0:T(8,128)S(1)} %get-tuple-element.393, f32[2,4,8,32]{3,1,2,0:T(4,128)S(1)} %bitcast.94, pred[8,32,256]{2,1,0:T(8,128)(4,1)S(1)} %fusion.48), kind=kLoop, calls=%fused_computation.9.clone.1 | loop fusion | flops 2095104 | bytes 3227648 | tf_op jit(solution)/shard_map/reshape.263
  58.3 0.7 fusion.52
  59.4 0.1 fusion.48
  59.6 1.7 %fusion.49 = (f32[2,4,8,32]{3,1,2,0:T(4,128)S(1)}, f32[1,2,4,8,32,256]{5,4,2,3,1,0:T(8,128)S(1)}) fusion(f32[8,32,256]{2,1,0:T(8,128)S(1)} %subtract_convert_fusion.2, f32[2,4]{1,0:T(2,128)S(1)} %mul.331, bf16[1,8,32,2,4,64]{5,2,4,1,3,0:T(8,128)(2,1)} %get-tuple-element.431, bf16[1,1024,2,64]{1,3,2,0:T(8,128)(2,1)} %get-tuple-element.430, ...), kind=kOutput, calls=%fused_computation.58.clone.1 | convolution fusion | flops 70252544 | bytes 3022884 | tf_op jit(solution)/shard_map/while/body/eval_jaxpr/sbqkgd,snkd->skgbqn/dot_general | solution.py:78
  61.4 0.8 %fusion.51 = (bf16[2,4,8,32,256]{4,3,1,2,0:T(8,128)(2,1)S(1)}, f32[2,4,8,32]{3,1,2,0:T(4,128)S(1)}) fusion(f32[1,2,4,8,32,256]{5,4,2,3,1,0:T(8,128)S(1)} %get-tuple-element.393, f32[2,4,8,32]{3,1,2,0:T(4,128)S(1)} %bitcast.94, pred[8,32,256]{2,1,0:T(8,128)(4,1)S(1)} %fusion.48), kind=kLoop, calls=%fused_computation.9.clone.1 | loop fusion | flops 2095104 | bytes 3227648 | tf_op jit(solution)/shard_map/reshape.263
  62.3 0.7 fusion.52
  63.0 0.3 fusion.26
  63.3 0.4 copy.50
  63.8 0.3 convert_element_type.92
  64.2 1.2 %fusion.19 = bf16[1024,256]{0,1:T(8,128)(2,1)} fusion(bf16[256,512]{1,0:T(8,128)(2,1)S(1)} %convert_element_type.92, bf16[512,1024]{1,0:T(8,128)(2,1)S(1)} %copy-done.1), kind=kOutput, calls=%fused_computation.38 | convolution fusion | flops 268697600 | bytes 1835008 | tf_op jit(solution)/shard_map/dot_general | solution.py:140
  65.5 0.7 reshape.338
  66.2 8.4 %reduce-scatter.2.cloned.1.call-done = bf16[512,256]{0,1:T(8,128)(2,1)} async-done(((bf16[1024,256]{0,1:T(8,128)(2,1)}), bf16[512,256]{0,1:T(8,128)(2,1)}) %reduce-scatter.2.cloned.1.call-update) | async-done | bytes 262160 | tf_op jit(solution)/shard_map/reduce_scatter | solution.py:142
  (76 shorter events, 2.5 us)
Async XLA Ops:
  7.2 35.7 %copy-start = (bf16[1024,512]{1,0:T(8,128)(2,1)S(1)}, bf16[1024,512]{1,0:T(8,128)(2,1)}, u32[]{:S(2)}) copy-start(bf16[1024,512]{1,0:T(8,128)(2,1)} %param.13) | copy-start | bytes 3145732
  7.2 4.3 %copy-start.3 = (f32[1024]{0:T(1024)S(1)}, f32[1024]{0:T(1024)}, u32[]{:S(2)}) copy-start(f32[1024]{0:T(1024)} %param.12) | copy-start | bytes 12292
  7.2 4.3 %copy-start.6 = (bf16[1024,128]{1,0:T(8,128)(2,1)S(1)}, bf16[1024,128]{1,0:T(8,128)(2,1)}, u32[]{:S(2)}) copy-start(bf16[1024,128]{1,0:T(8,128)(2,1)} %param.14) | copy-start | bytes 786436
  7.2 4.8 %copy-start.4 = (f32[64]{0:T(128)S(1)}, f32[64]{0:T(128)}, u32[]{:S(2)}) copy-start(f32[64]{0:T(128)} %param.17) | copy-start | bytes 772
  7.2 67.3 %reduce-scatter.2.cloned.1.call-start = ((), (), s32[]{:S(2)}) async-start(), calls=%async_computation.1 | async-start | bytes 786432 | tf_op jit(solution)/shard_map/reduce_scatter | solution.py:142
  44.2 2.0 %copy-start.5 = (f32[64]{0:T(128)S(1)}, f32[64]{0:T(128)}, u32[]{:S(2)}) copy-start(f32[64]{0:T(128)} %param.16) | copy-start | bytes 772
  44.4 2.9 %copy-start.2 = (s32[1,8,16]{2,1,0:T(8,128)S(1)}, s32[1,8,16]{2,1,0:T(8,128)}, u32[]{:S(2)}) copy-start(s32[1,8,16]{2,1,0:T(8,128)} %param.19) | copy-start | bytes 1540
  63.0 1.2 %copy-start.1 = (bf16[512,1024]{1,0:T(8,128)(2,1)S(1)}, bf16[512,1024]{1,0:T(8,128)(2,1)}, u32[]{:S(2)}) copy-start(bf16[512,1024]{1,0:T(8,128)(2,1)} %param.18) | copy-start | bytes 3145732
Sparse Core Ops, SparseCore 0:
  65.6 8.9 reduce-scatter.1
